TPU v7x, 32 devices: a whole 2x2x4 slice. The times are simulated.
32 devices in a mesh: ep: 16 (over z, y, x), tp: 2 (over core).
Axes of the slice: x: 2, y: 2, z: 4, core: 2. Of those that a mesh axis runs over, the one named last changes fastest.
Arguments:
- tokens: bfloat16 [512, 2048], P('ep'), may hold values from -6 to 6
- lru_state: float32 [512, 1024], P('ep', 'tp'), may hold values from -6 to 6
- conv_window: bfloat16 [512, 3, 1024], P('ep', None, 'tp'), may hold values from -6 to 6
- gain_mix_in: float32 [2048], replicated, may hold values from 0.1 to 1.9
- gain_mix_out: float32 [2048], replicated, may hold values from 0.1 to 1.9
- gain_ffn_in: float32 [2048], replicated, may hold values from 0.1 to 1.9
- gain_ffn_out: float32 [2048], replicated, may hold values from 0.1 to 1.9
- w_branch: bfloat16 [2048, 1024], P(None, 'tp'), may hold values from -0.125 to 0.125
- w_input: bfloat16 [2048, 1024], P(None, 'tp'), may hold values from -0.125 to 0.125
- conv_taps: bfloat16 [4, 1024], P(None, 'tp'), may hold values from -3 to 3
- gate_a: bfloat16 [8, 128, 128], P('tp'), may hold values from -0.5 to 0.5
- gate_x: bfloat16 [8, 128, 128], P('tp'), may hold values from -0.5 to 0.5
- decay_rate: float32 [1024], P('tp'), may hold values from 0.001 to 0.3
- w_mix_out: bfloat16 [1024, 2048], P('tp'), may hold values from -0.1875 to 0.1875
- routes: int32 [512, 4], P('ep'), may hold values from 0 to 15, all different within a row; in each aligned block of 32 rows (0 to 31, 32 to 63, ...) at most 16 rows name the same one
- route_weight: float32 [512, 4], P('ep'), may hold values from 0.2 to 1.5
- expert_gate: bfloat16 [16, 2048, 512], P('ep', None, 'tp'), may hold values from -0.125 to 0.125
- expert_up: bfloat16 [16, 2048, 512], P('ep', None, 'tp'), may hold values from -0.125 to 0.125
- expert_down: bfloat16 [16, 512, 2048], P('ep', 'tp'), may hold values from -0.25 to 0.25
- shared_gate: bfloat16 [2048, 512], P(None, 'tp'), may hold values from -0.125 to 0.125
- shared_up: bfloat16 [2048, 512], P(None, 'tp'), may hold values from -0.125 to 0.125
- shared_down: bfloat16 [512, 2048], P('tp'), may hold values from -0.25 to 0.25
Outputs:
- layer_out: bfloat16 [512, 2048], P('ep')
- new_state: float32 [512, 1024], P('ep', 'tp')
- new_window: bfloat16 [512, 3, 1024], P('ep', None, 'tp')
Inputs may be any that keep to these rules, and one draw needn't show every extreme that they name: `routes`: each row names 4 different experts. Within the rows of one device (aligned blocks of 32 rows) no expert is named by more than 16 entries, a bound that some block reaches.
All inputs are finite; a program needn't handle non-finite values.
Results may differ from a plain program's by a relative error of at most 0.014.
Values may be sent and summed in bfloat16 or wider, within the bound.
A program may use at most 64 MiB of HBM per device.

v0:
```python
import jax
import jax.numpy as jnp
from jax import lax
from jax.sharding import PartitionSpec as P


def rms_norm(value, gain):
    return value * lax.rsqrt(jnp.mean(value * value, axis=-1, keepdims=True) + 1e-06) * gain


def rounded_term(value):
    return lax.optimization_barrier(value.astype(jnp.bfloat16)).astype(jnp.float32)


def on_device(
    tokens,
    lru_state,
    conv_window,
    gain_mix_in,
    gain_mix_out,
    gain_ffn_in,
    gain_ffn_out,
    w_branch,
    w_input,
    conv_taps,
    gate_a,
    gate_x,
    decay_rate,
    w_mix_out,
    routes,
    route_weight,
    expert_gate,
    expert_up,
    expert_down,
    shared_gate,
    shared_up,
    shared_down,
):
    resid = tokens.astype(jnp.float32)
    normed = rms_norm(resid, gain_mix_in).astype(jnp.bfloat16)
    branch = jnp.dot(normed, w_branch, preferred_element_type=jnp.float32)
    inflow = jnp.dot(normed, w_input, preferred_element_type=jnp.float32).astype(jnp.bfloat16)
    window = jnp.concatenate([conv_window, inflow[:, None, :]], axis=1)
    new_window = window[:, 1:]
    conv = jnp.sum(window.astype(jnp.float32) * conv_taps.astype(jnp.float32)[None], axis=1)
    count, local_ch = conv.shape
    groups, group_dim = (gate_a.shape[0], gate_a.shape[1])
    grouped = conv.astype(jnp.bfloat16).reshape(count, groups, group_dim)
    recur_gate = jax.nn.sigmoid(
        jnp.einsum("sbi,bij->sbj", grouped, gate_a, preferred_element_type=jnp.float32).reshape(
            count, local_ch
        )
    )
    input_gate = jax.nn.sigmoid(
        jnp.einsum("sbi,bij->sbj", grouped, gate_x, preferred_element_type=jnp.float32).reshape(
            count, local_ch
        )
    )
    log_decay = -8.0 * recur_gate * decay_rate[None]
    new_state = (
        jnp.exp(log_decay) * lru_state + jnp.sqrt(-jnp.expm1(2.0 * log_decay)) * conv * input_gate
    )
    gated = (new_state * jax.nn.gelu(branch)).astype(jnp.bfloat16)
    mix_term = rounded_term(jnp.dot(gated, w_mix_out, preferred_element_type=jnp.float32))
    mixed = lax.psum(mix_term.astype(jnp.bfloat16), "tp").astype(jnp.float32)
    middle = (resid + rms_norm(mixed, gain_mix_out)).astype(jnp.bfloat16)
    ffn_in = rms_norm(middle.astype(jnp.float32), gain_ffn_in).astype(jnp.bfloat16)
    width = ffn_in.shape[1]
    top = routes.shape[1]
    local_exp = expert_gate.shape[0]
    experts = local_exp * lax.axis_size("ep")
    capacity = max(2, 2 * count * top // experts)
    flat = routes.reshape(count * top)
    onehot = (flat[:, None] == jnp.arange(experts, dtype=jnp.int32)[None, :]).astype(jnp.int32)
    rank = jnp.sum(onehot * (jnp.cumsum(onehot, axis=0) - 1), axis=-1)
    dest = flat * capacity + rank
    slot_ids = jnp.arange(experts * capacity, dtype=jnp.int32)
    placed = jnp.any(dest.reshape(count, top)[None, :, :] == slot_ids[:, None, None], axis=-1)
    outbound = jnp.dot(placed.astype(jnp.bfloat16), ffn_in, preferred_element_type=jnp.float32)
    outbound = outbound.astype(jnp.bfloat16).reshape(experts, capacity, width)
    shared_hidden = (
        jax.nn.silu(jnp.dot(ffn_in, shared_gate, preferred_element_type=jnp.float32))
        * jnp.dot(ffn_in, shared_up, preferred_element_type=jnp.float32)
    ).astype(jnp.bfloat16)
    shared = lax.psum(
        rounded_term(
            jnp.dot(shared_hidden, shared_down, preferred_element_type=jnp.float32)
        ).astype(jnp.bfloat16),
        "tp",
    ).astype(jnp.float32)
    share = width // lax.axis_size("tp")
    own = lax.dynamic_slice_in_dim(outbound, lax.axis_index("tp") * share, share, 2)
    arrived = lax.all_to_all(own, "ep", split_axis=0, concat_axis=1, tiled=True)
    rows = lax.all_gather(arrived, "tp", axis=2, tiled=True)
    hidden = (
        jax.nn.silu(
            jnp.einsum("erd,edf->erf", rows, expert_gate, preferred_element_type=jnp.float32)
        )
        * jnp.einsum("erd,edf->erf", rows, expert_up, preferred_element_type=jnp.float32)
    ).astype(jnp.bfloat16)
    summed = lax.psum_scatter(
        rounded_term(
            jnp.einsum("erf,efd->erd", hidden, expert_down, preferred_element_type=jnp.float32)
        ).astype(jnp.bfloat16),
        "tp",
        scatter_dimension=2,
        tiled=True,
    )
    back = lax.all_to_all(summed, "ep", split_axis=1, concat_axis=0, tiled=True)
    flat_out = back.reshape(experts * capacity, share)
    picked = flat_out[dest].reshape(count, top, flat_out.shape[1])
    routed_share = jnp.sum(picked.astype(jnp.float32) * route_weight[:, :, None], axis=1).astype(
        jnp.bfloat16
    )
    routed = lax.all_gather(routed_share, "tp", axis=1, tiled=True)
    total = routed.astype(jnp.float32) + shared
    layer_out = (middle.astype(jnp.float32) + rms_norm(total, gain_ffn_out)).astype(jnp.bfloat16)
    return (layer_out, new_state, new_window)


def solution(mesh):
    placed = (
        P("ep", None),
        P("ep", "tp"),
        P("ep", None, "tp"),
        P(),
        P(),
        P(),
        P(),
        P(None, "tp"),
        P(None, "tp"),
        P(None, "tp"),
        P("tp", None, None),
        P("tp", None, None),
        P("tp"),
        P("tp", None),
        P("ep", None),
        P("ep", None),
        P("ep", None, "tp"),
        P("ep", None, "tp"),
        P("ep", "tp", None),
        P(None, "tp"),
        P(None, "tp"),
        P("tp", None),
    )
    return jax.shard_map(
        on_device,
        mesh=mesh,
        in_specs=placed,
        out_specs=(P("ep", None), P("ep", "tp"), P("ep", None, "tp")),
        check_vma=False,
    )
```

profile of v0, /device:TPU:0, one launch (start us, length us, event | category | flops | bytes accessed | tf_op | source)
XLA Modules:
  0.0 134.1 jit_solution(11292914418998984690)
XLA Ops:
  7.3 1.2 fusion.24
  9.2 2.2 %fusion.10 = bf16[32,1,512]{2,0,1:T(8,128)(2,1)S(1)} fusion(bf16[2048,512]{1,0:T(8,128)(2,1)} %param.30, bf16[32,2048]{1,0:T(8,128)(2,1)} %param.22, f32[2048]{0:T(1024)} %param.25, f32[32]{0:T(128)S(1)} %add_rsqrt_fusion.3), kind=kOutput, calls=%fused_computation.19 | convolution fusion | flops 67387392 | bytes 2269312 | tf_op jit(solution)/shard_map/dot_general | solution.py:42
  12.0 3.2 %convolution_convert_fusion.3 = bf16[32,2048]{1,0:T(8,128)(2,1)} fusion(bf16[512,2048]{1,0:T(8,128)(2,1)S(1)} %copy-done, f32[32,512]{1,0:T(8,128)S(1)} %fusion.49, bf16[2048,512]{1,0:T(8,128)(2,1)} %param.29, bf16[32,2048]{1,0:T(8,128)(2,1)S(1)} %copy-done.2, f32[2048]{0:T(1024)S(1)} %copy-done.10, f32[32]{0:T(128)S(1)} %add_rsqrt_fusion.3), kind=kOutput, calls=%fused_computation.5 | convolution fusion | flops 134709248 | bytes 4530304 | tf_op jit(solution)/shard_map/dot_general | solution.py:64
  16.9 19.2 %all-reduce.3.cloned.1.call-done = bf16[32,2048]{1,0:T(8,128)(2,1)} async-done(((bf16[32,2048]{1,0:T(8,128)(2,1)}), bf16[32,2048]{1,0:T(8,128)(2,1)}) %all-reduce.3.cloned.1.call-update) | async-done | bytes 131088 | tf_op jit(solution)/shard_map/psum | solution.py:65
  36.1 1.0 fusion.22
  37.1 1.1 fusion.28
  38.9 22.2 %all_to_all.21 = bf16[16,16,1024]{2,1,0:T(8,128)(2,1)} all-to-all(bf16[16,16,1024]{2,1,0:T(8,128)(2,1)S(1)} %constant_dynamic-slice_fusion), channel_id=1, replica_groups=mesh['ep'=16,'tp'=2] {'ep'}, dimensions={0} | all-to-all | bytes 1048576 | tf_op jit(solution)/shard_map/all_to_all | solution.py:93
  61.1 7.5 %all-gather.2.cloned.1.call-done = bf16[1,256,2048]{2,1,0:T(8,128)(2,1)} async-done(((bf16[1,256,1024]{2,1,0:T(8,128)(2,1)}), bf16[1,256,2048]{2,1,0:T(8,128)(2,1)}) %all-gather.2.cloned.1.call-update) | async-done | bytes 1048592 | tf_op jit(solution)/shard_map/all_gather | solution.py:94
  68.6 2.1 %fusion.14 = f32[256,256]{1,0:T(8,128)S(1)} fusion(bf16[1,2048,256]{2,1,0:T(8,128)(2,1)} %param.38, bf16[1,256,2048]{2,1,0:T(8,128)(2,1)} %all-gather.2.cloned.1.call-done), kind=kOutput, calls=%fused_computation.24 | convolution fusion | flops 268435456 | bytes 2359296 | tf_op jit(solution)/shard_map/erd,edf->erf/dot_general | solution.py:97
  70.7 3.8 %fusion = bf16[1,256,2048]{2,1,0:T(8,128)(2,1)} fusion(bf16[1,256,2048]{2,1,0:T(8,128)(2,1)} %param.40, bf16[1,2048,256]{2,1,0:T(8,128)(2,1)} %param.39, bf16[1,256,2048]{2,1,0:T(8,128)(2,1)S(1)} %copy-done.1, f32[256,256]{1,0:T(8,128)S(1)} %fusion.14), kind=kOutput, calls=%fused_computation.3 | convolution fusion | flops 537788416 | bytes 4456448 | tf_op jit(solution)/shard_map/erf,efd->erd/dot_general | solution.py:103
  76.2 8.1 %reduce-scatter.2.cloned.1.call-done = bf16[1,256,1024]{2,1,0:T(8,128)(2,1)} async-done(((bf16[1,256,2048]{2,1,0:T(8,128)(2,1)}), bf16[1,256,1024]{2,1,0:T(8,128)(2,1)}) %reduce-scatter.2.cloned.1.call-update) | async-done | bytes 524304 | tf_op jit(solution)/shard_map/reduce_scatter | solution.py:101
  84.3 1.9 %copy.81 = bf16[1,256,1024]{2,0,1:T(2,128)(2,1)S(1)} copy(bf16[1,256,1024]{2,1,0:T(8,128)(2,1)} %reduce-scatter.2.cloned.1.call-done) | data formatting | bytes 1048576 | tf_op jit(solution)/shard_map/reduce_scatter | solution.py:101
  86.7 4.5 %reduce = bf16[256,1024]{1,0:T(8,128)(2,1)} reduce(bf16[256,1,1024]{2,1,0:T(2,128)(2,1)S(1)} %bitcast.73, bf16[]{:T(256)} %broadcast.143), dimensions={1}, to_apply=%bitcast.70.reduce_sub_computation | reduce | bytes 1048578
  91.2 2.2 %reshape.155 = bf16[16,2,8192]{2,1,0:T(2,128)(2,1)} reshape(bf16[256,1024]{1,0:T(8,128)(2,1)} %reduce) | data formatting | bytes 1048576
  93.4 6.8 %all-to-all-start.1 = ((bf16[16,2,8192]{2,1,0:T(2,128)(2,1)}), bf16[16,2,8192]{2,1,0:T(2,128)(2,1)S(1)}, u32[]{:S(2)}, u32[]{:S(2)}) async-start(bf16[16,2,8192]{2,1,0:T(2,128)(2,1)} %reshape.155), calls=%async_computation.2 | async-start | bytes 1048576 | tf_op jit(solution)/shard_map/all_to_all | solution.py:109
  100.9 1.5 %fusion.82 = f32[32,256]{1,0:T(8,128)S(1)} fusion(bf16[2048,256]{1,0:T(8,128)(2,1)} %param.41, bf16[32,2048]{1,0:T(8,128)(2,1)S(1)} %get-tuple-element.4, f32[2048]{0:T(1024)S(1)} %copy-done.8, f32[32]{0:T(128)S(1)} %add_rsqrt_fusion.1), kind=kOutput, calls=%fused_computation.113 | convolution fusion | flops 33816576 | bytes 1220736 | tf_op jit(solution)/shard_map/dot_general | solution.py:82
  102.5 3.0 %convolution_convert_fusion.2 = bf16[32,2048]{1,0:T(8,128)(2,1)} fusion(bf16[256,2048]{1,0:T(8,128)(2,1)} %param.43, bf16[2048,256]{1,0:T(8,128)(2,1)} %param.42, f32[32,256]{1,0:T(8,128)S(1)} %fusion.82, bf16[32,2048]{1,0:T(8,128)(2,1)S(1)} %get-tuple-element.4, f32[2048]{0:T(1024)S(1)} %copy-done.8, f32[32]{0:T(128)S(1)} %add_rsqrt_fusion.1), kind=kOutput, calls=%fused_computation.4 | convolution fusion | flops 67485696 | bytes 2400384 | tf_op jit(solution)/shard_map/dot_general | solution.py:87
  105.5 10.2 %all-to-all-done.1 = bf16[16,2,8192]{2,1,0:T(2,128)(2,1)S(1)} async-done(((bf16[16,2,8192]{2,1,0:T(2,128)(2,1)}), bf16[16,2,8192]{2,1,0:T(2,128)(2,1)S(1)}, u32[]{:S(2)}, u32[]{:S(2)}) %all-to-all-start.1) | async-done | bytes 524320 | tf_op jit(solution)/shard_map/all_to_all | solution.py:109
  115.7 1.8 %reshape.156 = bf16[256,1,1024]{2,1,0:T(2,128)(2,1)} reshape(bf16[16,2,8192]{2,1,0:T(2,128)(2,1)S(1)} %all-to-all-done.1) | data formatting | bytes 1048576
  117.4 1.4 %copy.80 = bf16[1,256,1024]{2,1,0:T(8,128)(2,1)S(1)} copy(bf16[1,256,1024]{2,0,1:T(2,128)(2,1)} %bitcast.72) | data formatting | bytes 1048576
  120.3 1.9 %all_gather.7 = bf16[32,2048]{1,0:T(8,128)(2,1)S(1)} all-gather(bf16[32,1024]{1,0:T(8,128)(2,1)S(1)} %multiply_reduce_fusion), channel_id=1, replica_groups=mesh['ep'=16,'tp'=2] {'tp'}, dimensions={1}, use_global_device_ids=true | all-gather | bytes 196608 | tf_op jit(solution)/shard_map/all_gather | solution.py:115
  122.2 2.7 %all-reduce.5.cloned.1.call-done = bf16[32,2048]{1,0:T(8,128)(2,1)} async-done(((bf16[32,2048]{1,0:T(8,128)(2,1)}), bf16[32,2048]{1,0:T(8,128)(2,1)}) %all-reduce.5.cloned.1.call-update) | async-done | bytes 131088 | tf_op jit(solution)/shard_map/psum | solution.py:85
  124.8 1.1 multiply_reduce_fusion.1
  125.9 1.7 %fusion.31 = bf16[32,2048]{1,0:T(8,128)(2,1)} fusion(bf16[32,2048]{1,0:T(8,128)(2,1)S(1)} %get-tuple-element.4, bf16[32,2048]{1,0:T(8,128)(2,1)} %all-reduce.5.cloned.1.call-done, bf16[32,2048]{1,0:T(8,128)(2,1)S(1)} %all_gather.7, f32[2048]{0:T(1024)S(1)} %copy-done.11, f32[32]{0:T(128)S(1)} %add_rsqrt_fusion), kind=kLoop, calls=%fused_computation.47 | loop fusion | flops 524288 | bytes 532608 | tf_op jit(solution)/shard_map/convert_element_type | solution.py:117
  (72 shorter events, 7.7 us)
Async XLA Ops:
  7.2 4.8 %copy-start = (bf16[512,2048]{1,0:T(8,128)(2,1)S(1)}, bf16[512,2048]{1,0:T(8,128)(2,1)}, u32[]{:S(2)}) copy-start(bf16[512,2048]{1,0:T(8,128)(2,1)} %param.35) | copy-start | bytes 6291460
  7.2 4.8 %copy-start.2 = (bf16[32,2048]{1,0:T(8,128)(2,1)S(1)}, bf16[32,2048]{1,0:T(8,128)(2,1)}, u32[]{:S(2)}) copy-start(bf16[32,2048]{1,0:T(8,128)(2,1)} %param.22) | copy-start | bytes 393220
  7.2 4.8 %copy-start.10 = (f32[2048]{0:T(1024)S(1)}, f32[2048]{0:T(1024)}, u32[]{:S(2)}) copy-start(f32[2048]{0:T(1024)} %param.25) | copy-start | bytes 24580
  7.2 4.2 %copy-start.3 = (bf16[32,3,512]{2,0,1:T(8,128)(2,1)S(1)}, bf16[32,3,512]{2,0,1:T(8,128)(2,1)}, u32[]{:S(2)}) copy-start(bf16[32,3,512]{2,0,1:T(8,128)(2,1)} %param.24) | copy-start | bytes 294916
  7.2 4.2 %copy-start.15 = (bf16[4,128,128]{2,1,0:T(8,128)(2,1)S(1)}, bf16[4,128,128]{2,1,0:T(8,128)(2,1)}, u32[]{:S(2)}) copy-start(bf16[4,128,128]{2,1,0:T(8,128)(2,1)} %param.33) | copy-start | bytes 393220
  7.2 4.4 %copy-start.16 = (bf16[4,128,128]{2,1,0:T(8,128)(2,1)S(1)}, bf16[4,128,128]{2,1,0:T(8,128)(2,1)}, u32[]{:S(2)}) copy-start(bf16[4,128,128]{2,1,0:T(8,128)(2,1)} %param.32) | copy-start | bytes 393220
  7.2 4.6 %copy-start.14 = (f32[512]{0:T(512)S(1)}, f32[512]{0:T(512)}, u32[]{:S(2)}) copy-start(f32[512]{0:T(512)} %param.34) | copy-start | bytes 6148
  7.2 4.6 %copy-start.9 = (f32[32,512]{1,0:T(8,128)S(1)}, f32[32,512]{1,0:T(8,128)}, u32[]{:S(2)}) copy-start(f32[32,512]{1,0:T(8,128)} %param.23) | copy-start | bytes 196612
  7.3 28.8 %all-reduce.3.cloned.1.call-start = ((), (), s32[]{:S(2)}) async-start(), calls=%async_computation.3 | async-start | bytes 262144 | tf_op jit(solution)/shard_map/psum | solution.py:65
  11.4 3.8 %copy-start.5 = (bf16[32,1,512]{2,0,1:T(8,128)(2,1)}, bf16[32,1,512]{2,0,1:T(8,128)(2,1)S(1)}, u32[]{:S(2)}) copy-start(bf16[32,1,512]{2,0,1:T(8,128)(2,1)S(1)} %fusion.10) | copy-start | bytes 98308
  12.0 3.3 %copy-start.7 = (f32[32,512]{1,0:T(8,128)}, f32[32,512]{1,0:T(8,128)S(1)}, u32[]{:S(2)}) copy-start(f32[32,512]{1,0:T(8,128)S(1)} %fusion.49) | copy-start | bytes 196612
  12.0 3.4 %copy-start.13 = (s32[32,4]{0,1:T(4,128)S(1)}, s32[32,4]{0,1:T(4,128)}, u32[]{:S(2)}) copy-start(s32[32,4]{0,1:T(4,128)} %param.36) | copy-start | bytes 1540
  12.0 25.1 %copy-start.12 = (f32[2048]{0:T(1024)S(1)}, f32[2048]{0:T(1024)}, u32[]{:S(2)}) copy-start(f32[2048]{0:T(1024)} %param.26) | copy-start | bytes 24580
  12.0 26.3 %copy-start.8 = (f32[2048]{0:T(1024)S(1)}, f32[2048]{0:T(1024)}, u32[]{:S(2)}) copy-start(f32[2048]{0:T(1024)} %param.27) | copy-start | bytes 24580
  15.3 53.4 %all-gather.2.cloned.1.call-start = ((), (), s32[]{:S(2)}) async-start(), calls=%async_computation.4 | async-start | bytes 1572864 | tf_op jit(solution)/shard_map/all_gather | solution.py:94
  61.1 23.2 %reduce-scatter.2.cloned.1.call-start = ((), (), s32[]{:S(2)}) async-start(), calls=%async_computation.5 | async-start | bytes 1572864 | tf_op jit(solution)/shard_map/reduce_scatter | solution.py:101
  68.6 2.1 %copy-start.1 = (bf16[1,256,2048]{2,1,0:T(8,128)(2,1)S(1)}, bf16[1,256,2048]{2,1,0:T(8,128)(2,1)}, u32[]{:S(2)}) copy-start(bf16[1,256,2048]{2,1,0:T(8,128)(2,1)} %all-gather.2.cloned.1.call-done) | copy-start | bytes 3145732
  86.1 14.1 %copy-start.4 = (bf16[32,3,512]{2,0,1:T(8,128)(2,1)S(1)}, bf16[32,3,512]{2,0,1:T(8,128)(2,1)}, u32[]{:S(2)}) copy-start(bf16[32,3,512]{2,0,1:T(8,128)(2,1)} %param.24) | copy-start | bytes 294916
  86.2 14.1 %copy-start.6 = (bf16[32,1,512]{2,0,1:T(8,128)(2,1)S(1)}, bf16[32,1,512]{2,0,1:T(8,128)(2,1)}, u32[]{:S(2)}) copy-start(bf16[32,1,512]{2,0,1:T(8,128)(2,1)} %copy-done.5) | copy-start | bytes 98308
  93.4 22.3 %all-to-all-start.1 = ((bf16[16,2,8192]{2,1,0:T(2,128)(2,1)}), bf16[16,2,8192]{2,1,0:T(2,128)(2,1)S(1)}, u32[]{:S(2)}, u32[]{:S(2)}) async-start(bf16[16,2,8192]{2,1,0:T(2,128)(2,1)} %reshape.155), calls=%async_computation.2 | async-start | bytes 1048576 | tf_op jit(solution)/shard_map/all_to_all | solution.py:109
  100.2 24.7 %all-reduce.5.cloned.1.call-start = ((), (), s32[]{:S(2)}) async-start(), calls=%async_computation.6 | async-start | bytes 262144 | tf_op jit(solution)/shard_map/psum | solution.py:85
  118.8 7.1 %copy-start.11 = (f32[2048]{0:T(1024)S(1)}, f32[2048]{0:T(1024)}, u32[]{:S(2)}) copy-start(f32[2048]{0:T(1024)} %param.28) | copy-start | bytes 24580
Sparse Core Ops, SparseCore 0:
  15.4 20.6 all-reduce.2
  61.2 7.3 all-gather.1
  74.7 9.5 reduce-scatter.1
  105.6 19.1 all-reduce.4
where the time goes:
time: 135 us; the launch traced here: 134 us
  waiting for transfers between devices  47.7 us (35%)
  blocking collectives  24.1 us (18%)
  matrix products  16.7 us (12%)
  between operations  14.2 us (11%)
  other arithmetic  13.6 us (10%)
  local copies, waits for them, and re-layouts  10.9 us (8%)
  starting transfers between devices  6.93 us (5%)
    all_to_all x1, blocking collectives, on_device(): arrived = lax.all_to_all(own, 'ep', split_axis=0, concat_axis=1, tiled=True)  22.2 us
    psum x1, waiting for transfers between devices, on_device(): mixed = lax.psum(mix_term.astype(jnp.bfloat16), 'tp').astype(jnp.float32)  19.2 us
    all_to_all x1, waiting for transfers between devices, on_device(): back = lax.all_to_all(summed, 'ep', split_axis=1, concat_axis=0, tiled=True)  10.2 us
    reduce_scatter x1, waiting for transfers between devices, on_device(): lax.psum_scatter(rounded_term(jnp.einsum('erf,efd->erd', hidden, expert_d...  8.14 us
    all_gather x1, waiting for transfers between devices, on_device(): rows = lax.all_gather(arrived, 'tp', axis=2, tiled=True)  7.49 us
    unnamed x40, local copies, waits for them, and re-layouts  6.86 us
    all_to_all x1, starting transfers between devices, on_device(): back = lax.all_to_all(summed, 'ep', split_axis=1, concat_axis=0, tiled=True)  6.77 us
    unnamed x1, other arithmetic  4.5 us
  transfers between devices with their start and end apart: 5, of which 5 were waited for; matrix products, arithmetic and copies ran while one was open for 10% of the time, Pallas kernels for 0%

commit v1 on v0

v1 whole, which is shorter than its diff:
```python
import functools

import jax
import jax.numpy as jnp
from jax import lax
from jax.experimental import pallas as pl
from jax.experimental.pallas import tpu as pltpu
from jax.sharding import PartitionSpec as P

F32 = jnp.float32
BF16 = jnp.bfloat16


def rms_norm(value, gain):
    return value * lax.rsqrt(jnp.mean(value * value, axis=-1, keepdims=True) + 1e-06) * gain


def dot(a, b):
    return jnp.dot(a, b, preferred_element_type=F32)


def one_less_exp(value):
    series = 1.0 + value * (1.0 / 6.0)
    for term in (5.0, 4.0, 3.0, 2.0):
        series = 1.0 + value * (1.0 / term) * series
    return jnp.where(value > -0.1, -value * series, 1.0 - jnp.exp(value))


def kernel(
    n_ep,
    cap,
    tokens_h,
    lru_h,
    cw_h,
    g_mix_in,
    g_mix_out,
    g_ffn_in,
    g_ffn_out,
    wb_h,
    wi_h,
    taps,
    ga_h,
    gx_h,
    decay_rate,
    wm_h,
    routes,
    route_w,
    eg_h,
    eu_h,
    ed_h,
    sg_h,
    su_h,
    sd_h,
    out_ref,
    state_ref,
    inflow_ref,
    tokens,
    lru,
    cw,
    wb,
    wi,
    ga,
    gx,
    wm,
    eg,
    eu,
    ed,
    sg,
    su,
    sd,
    mix_mine,
    mix_other,
    sh_mine,
    sh_other,
    ffn,
    outb,
    rows,
    part,
    part_in,
    ret,
    back,
    routed,
    load_sem,
    pair_send,
    pair_recv,
    ep_send,
    ep_recv,
    fwd_send,
    fwd_recv,
    ret_send,
    ret_recv,
):
    me = lax.axis_index("ep")
    tp = lax.axis_index("tp")
    other = 1 - tp
    partner = {"tp": other}
    count, width = tokens.shape
    share = width // 2
    slots = n_ep * cap
    chunk = min(slots, 256)
    chunks = slots // chunk

    barrier = pltpu.get_barrier_semaphore()
    pl.semaphore_signal(barrier, inc=1, device_id=partner, device_id_type=pl.DeviceIdType.MESH)

    def greet(i, carry):
        pl.semaphore_signal(
            barrier,
            inc=1,
            device_id={"ep": lax.rem(me + i, n_ep)},
            device_id_type=pl.DeviceIdType.MESH,
        )
        return carry

    lax.fori_loop(1, n_ep, greet, 0)

    loads = []
    for i, (src, dst) in enumerate(
        (
            (tokens_h, tokens),
            (wb_h, wb),
            (wi_h, wi),
            (cw_h, cw),
            (ga_h, ga),
            (gx_h, gx),
            (lru_h, lru),
            (wm_h, wm),
            (sg_h, sg),
            (su_h, su),
            (sd_h, sd),
            (eg_h, eg),
            (eu_h, eu),
            (ed_h, ed),
        )
    ):
        copy = pltpu.make_async_copy(src, dst, load_sem.at[i])
        copy.start()
        loads.append(copy)
    (c_tok, c_wb, c_wi, c_cw, c_ga, c_gx, c_lru, c_wm, c_sg, c_su, c_sd, c_eg, c_eu, c_ed) = loads

    tri = (
        lax.broadcasted_iota(jnp.int32, (count, count), 0)
        > lax.broadcasted_iota(jnp.int32, (count, count), 1)
    ).astype(BF16)

    def slot_maps(first):
        place = first + lax.broadcasted_iota(jnp.int32, (count, chunk), 1)
        expert = place // cap
        slot = (place - expert * cap).astype(F32)
        named = jnp.zeros((count, chunk), F32)
        weight = jnp.zeros((count, chunk), F32)
        for k in range(routes.shape[1]):
            hit = routes[:, k : k + 1] == expert
            named = jnp.where(hit, 1.0, named)
            weight = jnp.where(hit, route_w[:, k : k + 1], weight)
        rank = dot(tri, named.astype(BF16))
        filled = (rank == slot) & (named > 0.0)
        return jnp.where(filled, 1.0, 0.0), jnp.where(filled, weight, 0.0)

    def over_chunks(body):
        if chunks == 1:
            body(0)
        else:
            lax.fori_loop(0, chunks, lambda i, c: (body(pl.multiple_of(i * chunk, chunk)), c)[1], 0)

    one_map = slot_maps(0) if chunks == 1 else None

    c_tok.wait()
    resid = tokens[...].astype(F32)
    normed = rms_norm(resid, g_mix_in[...]).astype(BF16)
    c_wi.wait()
    inflow = dot(normed, wi[...]).astype(BF16)
    inflow_ref[...] = inflow
    c_wb.wait()
    branch = dot(normed, wb[...])
    c_cw.wait()
    tap = taps[...].astype(F32)
    conv = inflow.astype(F32) * tap[3:4]
    for j in range(3):
        conv = conv + cw[j].astype(F32) * tap[j : j + 1]
    low = conv.astype(BF16)
    c_ga.wait()
    c_gx.wait()
    groups, group = ga.shape[0], ga.shape[1]
    pre_a, pre_x = [], []
    for g in range(groups):
        piece = low[:, g * group : (g + 1) * group]
        pre_a.append(dot(piece, ga[g]))
        pre_x.append(dot(piece, gx[g]))
    recur_gate = jax.nn.sigmoid(jnp.concatenate(pre_a, axis=1))
    input_gate = jax.nn.sigmoid(jnp.concatenate(pre_x, axis=1))
    log_decay = -8.0 * recur_gate * decay_rate[...]
    c_lru.wait()
    new_state = (
        jnp.exp(log_decay) * lru[...] + jnp.sqrt(one_less_exp(2.0 * log_decay)) * conv * input_gate
    )
    state_ref[...] = new_state
    gated = (new_state * jax.nn.gelu(branch)).astype(BF16)
    c_wm.wait()
    mix_mine[...] = dot(gated, wm[...]).astype(BF16)

    def pair(i, src, dst):
        return pltpu.make_async_remote_copy(
            src_ref=src,
            dst_ref=dst,
            send_sem=pair_send.at[i],
            recv_sem=pair_recv.at[i],
            device_id=partner,
            device_id_type=pl.DeviceIdType.MESH,
        )

    pl.semaphore_wait(barrier, n_ep)
    mix_copy = pair(0, mix_mine, mix_other)
    mix_copy.start()
    mix_copy.wait()
    mixed = mix_mine[...].astype(F32) + mix_other[...].astype(F32)
    middle = (resid + rms_norm(mixed, g_mix_out[...])).astype(BF16)
    ffn_in = rms_norm(middle.astype(F32), g_ffn_in[...]).astype(BF16)
    ffn[0] = ffn_in[:, :share]
    ffn[1] = ffn_in[:, share:]

    def fill(first):
        place = (one_map or slot_maps(first))[0]
        own = ffn[tp]
        outb[pl.ds(first, chunk), :] = lax.dot_general(
            place.astype(BF16), own, (((0,), (0,)), ((), ())), preferred_element_type=F32
        ).astype(BF16)

    over_chunks(fill)

    def block(i):
        return pl.ds(pl.multiple_of(i * cap, cap), cap)

    def to_ep(i):
        peer = lax.rem(me + i, n_ep)
        return pltpu.make_async_remote_copy(
            src_ref=outb.at[block(peer), :],
            dst_ref=rows.at[tp, block(me), :],
            send_sem=ep_send.at[i],
            recv_sem=ep_recv.at[i],
            device_id={"ep": peer},
            device_id_type=pl.DeviceIdType.MESH,
        )

    def forward(i):
        peer = lax.rem(me + n_ep - i, n_ep)
        place = rows.at[tp, block(peer), :]
        return pltpu.make_async_remote_copy(
            src_ref=place,
            dst_ref=place,
            send_sem=fwd_send.at[i],
            recv_sem=fwd_recv.at[i],
            device_id=partner,
            device_id_type=pl.DeviceIdType.MESH,
        )

    lax.fori_loop(1, n_ep, lambda i, c: (to_ep(i).start(), c)[1], 0)
    rows[tp, block(me), :] = outb[block(me), :]
    forward(0).start()

    c_sg.wait()
    c_su.wait()
    hidden = (jax.nn.silu(dot(ffn_in, sg[...])) * dot(ffn_in, su[...])).astype(BF16)
    c_sd.wait()
    sh_mine[...] = dot(hidden, sd[...]).astype(BF16)
    sh_copy = pair(1, sh_mine, sh_other)
    sh_copy.start()

    def relay(i, c):
        to_ep(i).wait_recv()
        forward(i).start()
        return c

    lax.fori_loop(1, n_ep, relay, 0)
    lax.fori_loop(0, n_ep, lambda i, c: (forward(i).wait(), c)[1], 0)

    c_eg.wait()
    c_eu.wait()
    c_ed.wait()
    mine_at = pl.ds(pl.multiple_of(tp * share, share), share)
    other_at = pl.ds(pl.multiple_of(other * share, share), share)

    def expert(first):
        at = pl.ds(first, chunk)
        low_rows, high_rows = rows[0, at, :], rows[1, at, :]
        gate = dot(low_rows, eg[:share]) + dot(high_rows, eg[share:])
        up = dot(low_rows, eu[:share]) + dot(high_rows, eu[share:])
        act = (jax.nn.silu(gate) * up).astype(BF16)
        part[at, :] = dot(act, ed[:, other_at]).astype(BF16)
        ret[at, :] = dot(act, ed[:, mine_at]).astype(BF16)

    over_chunks(expert)
    part_copy = pair(2, part, part_in)
    part_copy.start()
    part_copy.wait()

    def add(first):
        at = pl.ds(first, chunk)
        ret[at, :] = (ret[at, :].astype(F32) + part_in[at, :].astype(F32)).astype(BF16)

    over_chunks(add)

    def to_back(i):
        peer = lax.rem(me + i, n_ep)
        return pltpu.make_async_remote_copy(
            src_ref=ret.at[block(peer), :],
            dst_ref=back.at[block(me), :],
            send_sem=ret_send.at[i],
            recv_sem=ret_recv.at[i],
            device_id={"ep": peer},
            device_id_type=pl.DeviceIdType.MESH,
        )

    lax.fori_loop(1, n_ep, lambda i, c: (to_back(i).start(), c)[1], 0)
    back[block(me), :] = ret[block(me), :]
    sh_copy.wait()
    shared = sh_mine[...].astype(F32) + sh_other[...].astype(F32)
    lax.fori_loop(1, n_ep, lambda i, c: (to_back(i).wait(), c)[1], 0)

    def combined(first):
        weight = (one_map or slot_maps(first))[1]
        high = weight.astype(BF16)
        rest = (weight - high.astype(F32)).astype(BF16)
        landed = back[pl.ds(first, chunk), :]
        return dot(high, landed) + dot(rest, landed)

    if chunks == 1:
        sums = combined(0)
    else:
        sums = lax.fori_loop(
            0,
            chunks,
            lambda i, c: c + combined(pl.multiple_of(i * chunk, chunk)),
            jnp.zeros((count, share), F32),
        )
    routed[tp] = sums.astype(BF16)
    routed_copy = pair(3, routed.at[tp], routed.at[tp])
    routed_copy.start()
    routed_copy.wait()
    total = jnp.concatenate([routed[0], routed[1]], axis=1).astype(F32) + shared
    out_ref[...] = (middle.astype(F32) + rms_norm(total, g_ffn_out[...])).astype(BF16)
    lax.fori_loop(1, n_ep, lambda i, c: (to_ep(i).wait_send(), c)[1], 0)


def on_device(
    tokens,
    lru_state,
    conv_window,
    gain_mix_in,
    gain_mix_out,
    gain_ffn_in,
    gain_ffn_out,
    w_branch,
    w_input,
    conv_taps,
    gate_a,
    gate_x,
    decay_rate,
    w_mix_out,
    routes,
    route_weight,
    expert_gate,
    expert_up,
    expert_down,
    shared_gate,
    shared_up,
    shared_down,
):
    n_ep = lax.axis_size("ep")
    count, width = tokens.shape
    share = width // 2
    local_ch = lru_state.shape[1]
    capacity = max(2, 2 * count * routes.shape[1] // (n_ep * expert_gate.shape[0]))
    cap = -(-capacity // 16) * 16
    slots = n_ep * cap
    vmem = pl.BlockSpec(memory_space=pltpu.VMEM)
    hbm = pl.BlockSpec(memory_space=pl.ANY)
    window = jnp.transpose(conv_window, (1, 0, 2))
    args = (
        (tokens, hbm),
        (lru_state, hbm),
        (window, hbm),
        (gain_mix_in[None], vmem),
        (gain_mix_out[None], vmem),
        (gain_ffn_in[None], vmem),
        (gain_ffn_out[None], vmem),
        (w_branch, hbm),
        (w_input, hbm),
        (conv_taps, vmem),
        (gate_a, hbm),
        (gate_x, hbm),
        (decay_rate[None], vmem),
        (w_mix_out, hbm),
        (routes, vmem),
        (route_weight, vmem),
        (expert_gate[0], hbm),
        (expert_up[0], hbm),
        (expert_down[0], hbm),
        (shared_gate, hbm),
        (shared_up, hbm),
        (shared_down, hbm),
    )
    held = lambda a: pltpu.VMEM(a.shape, a.dtype)
    dma = pltpu.SemaphoreType.DMA
    layer_out, new_state, inflow = pl.pallas_call(
        functools.partial(kernel, n_ep, cap),
        out_shape=(
            jax.ShapeDtypeStruct((count, width), BF16),
            jax.ShapeDtypeStruct((count, local_ch), F32),
            jax.ShapeDtypeStruct((count, local_ch), BF16),
        ),
        in_specs=[spec for _, spec in args],
        out_specs=(vmem, vmem, vmem),
        scratch_shapes=[
            held(tokens),
            held(lru_state),
            held(window),
            held(w_branch),
            held(w_input),
            held(gate_a),
            held(gate_x),
            held(w_mix_out),
            held(expert_gate[0]),
            held(expert_up[0]),
            held(expert_down[0]),
            held(shared_gate),
            held(shared_up),
            held(shared_down),
            pltpu.VMEM((count, width), BF16),
            pltpu.VMEM((count, width), BF16),
            pltpu.VMEM((count, width), BF16),
            pltpu.VMEM((count, width), BF16),
            pltpu.VMEM((2, count, share), BF16),
            pltpu.VMEM((slots, share), BF16),
            pltpu.VMEM((2, slots, share), BF16),
            pltpu.VMEM((slots, share), BF16),
            pltpu.VMEM((slots, share), BF16),
            pltpu.VMEM((slots, share), BF16),
            pltpu.VMEM((slots, share), BF16),
            pltpu.VMEM((2, count, share), BF16),
            dma((14,)),
            dma((4,)),
            dma((4,)),
            dma((n_ep,)),
            dma((n_ep,)),
            dma((n_ep,)),
            dma((n_ep,)),
            dma((n_ep,)),
            dma((n_ep,)),
        ],
        compiler_params=pltpu.CompilerParams(
            collective_id=0, has_side_effects=True, vmem_limit_bytes=60 * 1024 * 1024
        ),
        name="layer",
    )(*[value for value, _ in args])
    new_window = jnp.concatenate([conv_window[:, 1:], inflow[:, None, :]], axis=1)
    return (layer_out, new_state, new_window)


def solution(mesh):
    placed = (
        P("ep", None),
        P("ep", "tp"),
        P("ep", None, "tp"),
        P(),
        P(),
        P(),
        P(),
        P(None, "tp"),
        P(None, "tp"),
        P(None, "tp"),
        P("tp", None, None),
        P("tp", None, None),
        P("tp"),
        P("tp", None),
        P("ep", None),
        P("ep", None),
        P("ep", None, "tp"),
        P("ep", None, "tp"),
        P("ep", "tp", None),
        P(None, "tp"),
        P(None, "tp"),
        P("tp", None),
    )
    return jax.shard_map(
        on_device,
        mesh=mesh,
        in_specs=placed,
        out_specs=(P("ep", None), P("ep", "tp"), P("ep", None, "tp")),
        check_vma=False,
    )
```

time: 135 us -> 49.8 us (0.37)
  the two profiles are of different devices: /device:TPU:0 before, /device:TPU:29 now
where the time goes in v1:
time: 49.8 us; the launch traced here: 49.5 us
  Pallas kernels  41.7 us (84%)
  local copies, waits for them, and re-layouts  5.78 us (12%)
  other arithmetic  1.41 us (3%)
  between operations  0.66 us (1%)
    pallas_call x1, Pallas kernels, on_device(): pl.pallas_call(functools.partial(kernel, n_ep, cap), out_shape=(jax.Shape...  41.7 us
    unnamed x6, local copies, waits for them, and re-layouts  5.78 us
    concatenate x1, other arithmetic, on_device(): jnp.concatenate([conv_window[:, 1:], inflow[:, None, :]], axis=1)  1.41 us

profile of v1, /device:TPU:29, one launch (start us, length us, event | category | flops | bytes accessed | tf_op | source)
XLA Modules:
  0.0 49.5 jit_solution(14513134937498845677)
XLA Ops:
  0.6 1.4 %copy.25.routes = s32[32,4]{1,0:T(8,128)} copy(s32[32,4]{0,1:T(4,128)} %param.36) | data formatting | bytes 1024 | tf_op args[14]
  2.0 1.4 %copy.26.route_w = f32[32,4]{1,0:T(8,128)} copy(f32[32,4]{0,1:T(4,128)} %param.37) | data formatting | bytes 1024 | tf_op args[15]
  3.4 0.0 copy-start
  3.4 41.7 %layer.1 = (bf16[32,2048]{1,0:T(8,128)(2,1)}, f32[32,512]{1,0:T(8,128)}, bf16[32,512]{1,0:T(8,128)(2,1)}) custom-call(bf16[32,2048]{1,0:T(8,128)(2,1)} %tokens_h.1, f32[32,512]{1,0:T(8,128)} %lru_h.1, bf16[3,32,512]{2,1,0:T(8,128)(2,1)} %bitcast.13, f32[1,2048]{1,0:T(1,128)} %bitcast.15, f32[1,2048]{1,0:T(1,128)} %bitcast.16, f32[1,2048]{1,0:T(1,128)} %bitcast.17, ...), custom_call_target="tpu_custom_call" | custom-call | tf_op jit(solution)/shard_map/layer/pallas_call | solution.py:405
  45.0 0.0 copy-done
  45.1 1.4 %pad_maximum_fusion = bf16[32,3,512]{2,0,1:T(8,128)(2,1)} fusion(bf16[32,1,512]{2,0,1:T(8,128)(2,1)} %bitcast.14, bf16[32,2,512]{2,0,1:T(8,128)(2,1)S(1)} %slice.3), kind=kLoop, calls=%fused_computation | loop fusion | flops 49152 | bytes 196608 | tf_op jit(solution)/shard_map/concatenate | solution.py:456
  46.5 1.6 %copy.29 = bf16[32,2048]{1,0:T(8,128)(2,1)} copy(bf16[32,2048]{1,0:T(8,128)(2,1)} %get-tuple-element.12) | data formatting | bytes 262144
  48.0 1.5 %copy.30 = f32[32,512]{1,0:T(8,128)} copy(f32[32,512]{1,0:T(8,128)} %get-tuple-element.13) | data formatting | bytes 131072
  (1 shorter events, 0.0 us)
Async XLA Ops:
  3.4 41.7 %copy-start = (bf16[32,3,512]{2,0,1:T(8,128)(2,1)S(1)}, bf16[32,3,512]{2,0,1:T(8,128)(2,1)}, u32[]{:S(2)}) copy-start(bf16[32,3,512]{2,0,1:T(8,128)(2,1)} %param.24) | copy-start | bytes 294916

commit v2 on v1

v2 whole, which is shorter than its diff:
```python
import functools

import jax
import jax.numpy as jnp
from jax import lax
from jax.experimental import pallas as pl
from jax.experimental.pallas import tpu as pltpu
from jax.sharding import PartitionSpec as P

F32 = jnp.float32
BF16 = jnp.bfloat16
MESH = pl.DeviceIdType.MESH


def rms_norm(value, gain):
    return value * lax.rsqrt(jnp.mean(value * value, axis=-1, keepdims=True) + 1e-06) * gain


def dot(a, b):
    return jnp.dot(a, b, preferred_element_type=F32)


def one_less_exp(value):
    series = 1.0 + value * (1.0 / 6.0)
    for term in (5.0, 4.0, 3.0, 2.0):
        series = 1.0 + value * (1.0 / term) * series
    return jnp.where(value > -0.1, -value * series, 1.0 - jnp.exp(value))


def kernel(
    outer,
    inner,
    cap,
    tokens_h,
    lru_h,
    cw_h,
    g_mix_in,
    g_mix_out,
    g_ffn_in,
    g_ffn_out,
    wb_h,
    wi_h,
    taps,
    ga_h,
    gx_h,
    decay_rate,
    wm_h,
    routes,
    route_w,
    eg_h,
    eu_h,
    ed_h,
    sg_h,
    su_h,
    sd_h,
    out_ref,
    state_ref,
    inflow_ref,
    tokens,
    lru,
    cw,
    wb,
    wi,
    ga,
    gx,
    wm,
    eg,
    eu,
    ed,
    sg,
    su,
    sd,
    mix_mine,
    mix_other,
    sh_mine,
    sh_other,
    ffn,
    info,
    line,
    outb,
    rows,
    part,
    part_in,
    kept,
    ret,
    back,
    sums,
    sums_in,
    own_sum,
    routed,
    load_sem,
    pair_send,
    pair_recv,
    ep_send,
    ep_recv,
    fwd_send,
    fwd_recv,
    ret_send,
    ret_recv,
    info_send,
    info_recv,
    line_send,
    line_recv,
    part_send,
    part_recv,
    sum_send,
    sum_recv,
):
    z, q = lax.axis_index("ep") // inner, lax.axis_index("ep") % inner
    tp = lax.axis_index("tp")
    other = 1 - tp
    partner = {"tp": other}
    count, width = tokens.shape
    share = width // 2
    order = sorted(range(1, outer), key=lambda j: -j)

    def from_z(j):
        place, bit = z, 1
        while bit <= j:
            if j & bit:
                place = place + bit - 2 * bit * (z // bit % 2)
            bit *= 2
        return place

    barrier = pltpu.get_barrier_semaphore()

    def greet(device):
        pl.semaphore_signal(barrier, inc=1, device_id=device, device_id_type=MESH)

    greet(partner)
    for j in range(1, outer):
        greet({"ep": from_z(j) * inner + q})
    lax.fori_loop(
        1, inner, lambda i, c: (greet({"ep": z * inner + lax.rem(q + i, inner)}), c)[1], 0
    )

    loads = []
    for i, (src, dst) in enumerate(
        (
            (tokens_h, tokens),
            (wb_h, wb),
            (wi_h, wi),
            (cw_h, cw),
            (ga_h, ga),
            (gx_h, gx),
            (lru_h, lru),
            (wm_h, wm),
            (sg_h, sg),
            (su_h, su),
            (sd_h, sd),
            (eg_h, eg),
            (eu_h, eu),
            (ed_h, ed),
        )
    ):
        copy = pltpu.make_async_copy(src, dst, load_sem.at[i])
        copy.start()
        loads.append(copy)
    (c_tok, c_wb, c_wi, c_cw, c_ga, c_gx, c_lru, c_wm, c_sg, c_su, c_sd, c_eg, c_eu, c_ed) = loads

    plane_rows = inner * cap
    earlier = (
        lax.broadcasted_iota(jnp.int32, (count, count), 0)
        < lax.broadcasted_iota(jnp.int32, (count, count), 1)
    ).astype(BF16)
    top = routes.shape[0]
    info[z] = jnp.zeros(info.shape[1:], F32)
    info[z, :top, :count] = routes[...].astype(F32)
    info[z, top : 2 * top, :count] = route_w[...]

    def slot_maps(block_z):
        place = lax.broadcasted_iota(jnp.int32, (plane_rows, count), 0)
        expert = place // cap
        slot = (place - expert * cap).astype(F32)
        expert = (expert + z * inner).astype(F32)
        named = jnp.zeros((plane_rows, count), F32)
        weight = jnp.zeros((plane_rows, count), F32)
        for k in range(top):
            hit = info[block_z, k : k + 1, :count] == expert
            named = jnp.where(hit, 1.0, named)
            weight = jnp.where(hit, info[block_z, top + k : top + k + 1, :count], weight)
        filled = (dot(named.astype(BF16), earlier) == slot) & (named > 0.0)
        return jnp.where(filled, 1.0, 0.0).astype(BF16), jnp.where(filled, weight, 0.0)

    c_tok.wait()
    resid = tokens[...].astype(F32)
    normed = rms_norm(resid, g_mix_in[...]).astype(BF16)
    c_wi.wait()
    inflow = dot(normed, wi[...]).astype(BF16)
    inflow_ref[...] = inflow
    c_wb.wait()
    branch = dot(normed, wb[...])
    c_cw.wait()
    tap = taps[...].astype(F32)
    conv = inflow.astype(F32) * tap[3:4]
    for j in range(3):
        conv = conv + cw[j].astype(F32) * tap[j : j + 1]
    low = conv.astype(BF16)
    c_ga.wait()
    c_gx.wait()
    groups, group = ga.shape[0], ga.shape[1]
    pre_a, pre_x = [], []
    for g in range(groups):
        piece = low[:, g * group : (g + 1) * group]
        pre_a.append(dot(piece, ga[g]))
        pre_x.append(dot(piece, gx[g]))
    recur_gate = jax.nn.sigmoid(jnp.concatenate(pre_a, axis=1))
    input_gate = jax.nn.sigmoid(jnp.concatenate(pre_x, axis=1))
    log_decay = -8.0 * recur_gate * decay_rate[...]
    c_lru.wait()
    new_state = (
        jnp.exp(log_decay) * lru[...] + jnp.sqrt(one_less_exp(2.0 * log_decay)) * conv * input_gate
    )
    state_ref[...] = new_state
    gated = (new_state * jax.nn.gelu(branch)).astype(BF16)
    c_wm.wait()
    mix_mine[...] = dot(gated, wm[...]).astype(BF16)

    def pair(i, src, dst):
        return pltpu.make_async_remote_copy(
            src_ref=src,
            dst_ref=dst,
            send_sem=pair_send.at[i],
            recv_sem=pair_recv.at[i],
            device_id=partner,
            device_id_type=MESH,
        )

    def on_line(src, dst, send, recv, j):
        return pltpu.make_async_remote_copy(
            src_ref=src.at[z],
            dst_ref=dst.at[z],
            send_sem=send.at[j],
            recv_sem=recv.at[j],
            device_id={"ep": from_z(j) * inner + q},
            device_id_type=MESH,
        )

    def info_copy(j):
        return on_line(info, info, info_send, info_recv, j)

    def line_copy(j):
        return on_line(line, line, line_send, line_recv, j)

    pl.semaphore_wait(barrier, outer + inner - 1)
    mix_copy = pair(0, mix_mine, mix_other)
    mix_copy.start()
    for j in order:
        info_copy(j).start()
    mix_copy.wait()
    mixed = mix_mine[...].astype(F32) + mix_other[...].astype(F32)
    middle = (resid + rms_norm(mixed, g_mix_out[...])).astype(BF16)
    ffn_in = rms_norm(middle.astype(F32), g_ffn_in[...]).astype(BF16)
    ffn[0] = ffn_in[:, :share]
    ffn[1] = ffn_in[:, share:]

    line[z] = ffn[tp]
    for j in order:
        line_copy(j).start()

    def block(i):
        return pl.ds(pl.multiple_of(i * cap, cap), cap)

    def at_plane(j, i):
        return block(from_z(j) * inner + lax.rem(i, inner))

    def to_ep(j, i):
        return pltpu.make_async_remote_copy(
            src_ref=outb.at[at_plane(j, q + i), :],
            dst_ref=rows.at[tp, at_plane(j, q), :],
            send_sem=ep_send.at[j * inner + i],
            recv_sem=ep_recv.at[j * inner + i],
            device_id={"ep": z * inner + lax.rem(q + i, inner)},
            device_id_type=MESH,
        )

    def forward(j, i):
        place = rows.at[tp, at_plane(j, q + inner - i), :]
        return pltpu.make_async_remote_copy(
            src_ref=place,
            dst_ref=place,
            send_sem=fwd_send.at[j * inner + i],
            recv_sem=fwd_recv.at[j * inner + i],
            device_id=partner,
            device_id_type=MESH,
        )

    def to_back(j, i):
        return pltpu.make_async_remote_copy(
            src_ref=ret.at[at_plane(j, q + i), :],
            dst_ref=back.at[at_plane(j, q), :],
            send_sem=ret_send.at[j * inner + i],
            recv_sem=ret_recv.at[j * inner + i],
            device_id={"ep": z * inner + lax.rem(q + i, inner)},
            device_id_type=MESH,
        )

    def rows_of(j):
        return pl.ds(pl.multiple_of(from_z(j) * plane_rows, plane_rows), plane_rows)

    def part_copy(j):
        return pltpu.make_async_remote_copy(
            src_ref=part.at[rows_of(j), :],
            dst_ref=part_in.at[rows_of(j), :],
            send_sem=part_send.at[j],
            recv_sem=part_recv.at[j],
            device_id=partner,
            device_id_type=MESH,
        )

    def sum_copy(j):
        return pltpu.make_async_remote_copy(
            src_ref=sums.at[j],
            dst_ref=sums_in.at[j],
            send_sem=sum_send.at[j],
            recv_sem=sum_recv.at[j],
            device_id={"ep": from_z(j) * inner + q},
            device_id_type=MESH,
        )

    def each(first, body):
        lax.fori_loop(first, inner, lambda i, c: (body(i), c)[1], 0)

    weights = {}

    def send_rows(j):
        if j > 0:
            info_copy(j).wait_recv()
            line_copy(j).wait_recv()
        place, weights[j] = slot_maps(from_z(j))
        outb[rows_of(j), :] = dot(place, line[from_z(j)]).astype(BF16)
        each(1, lambda i: to_ep(j, i).start())
        rows[tp, at_plane(j, q), :] = outb[at_plane(j, q), :]
        forward(j, 0).start()

    def relay_rows(j):
        def one(i):
            to_ep(j, i).wait_recv()
            forward(j, i).start()

        each(1, one)

    mine_at = pl.ds(pl.multiple_of(tp * share, share), share)
    other_at = pl.ds(pl.multiple_of(other * share, share), share)

    def run_expert(j):
        if j == 0:
            c_eg.wait()
            c_eu.wait()
            c_ed.wait()
        each(0, lambda i: forward(j, i).wait_recv())
        low_rows, high_rows = rows[0, rows_of(j), :], rows[1, rows_of(j), :]
        gate = dot(low_rows, eg[:share]) + dot(high_rows, eg[share:])
        up = dot(low_rows, eu[:share]) + dot(high_rows, eu[share:])
        act = (jax.nn.silu(gate) * up).astype(BF16)
        part[rows_of(j), :] = dot(act, ed[:, other_at]).astype(BF16)
        part_copy(j).start()
        kept[rows_of(j), :] = dot(act, ed[:, mine_at]).astype(BF16)

    def send_back(j):
        part_copy(j).wait_recv()
        ret[rows_of(j), :] = (
            kept[rows_of(j), :].astype(F32) + part_in[rows_of(j), :].astype(F32)
        ).astype(BF16)
        each(1, lambda i: to_back(j, i).start())
        back[at_plane(j, q), :] = ret[at_plane(j, q), :]

    def weigh(j):
        each(1, lambda i: to_back(j, i).wait_recv())
        high = weights[j].astype(BF16)
        rest = (weights[j] - high.astype(F32)).astype(BF16)
        landed = back[rows_of(j), :]
        turned = lambda w: lax.dot_general(
            w, landed, (((0,), (0,)), ((), ())), preferred_element_type=F32
        )
        partial = turned(high) + turned(rest)
        if j == 0:
            own_sum[...] = partial
        else:
            sums[j] = partial.astype(BF16)
            sum_copy(j).start()

    sh_copy = pair(1, sh_mine, sh_other)
    for step in range(outer + 5):
        for stage, lag in ((send_rows, 0), (send_back, 3), (run_expert, 2), (relay_rows, 1), (weigh, 5)):
            if 0 <= step - lag < outer:
                stage(step - lag)
        if step == 0:
            c_sg.wait()
            c_su.wait()
            hidden = (jax.nn.silu(dot(ffn_in, sg[...])) * dot(ffn_in, su[...])).astype(BF16)
            c_sd.wait()
            sh_mine[...] = dot(hidden, sd[...]).astype(BF16)
            sh_copy.start()

    sh_copy.wait()
    shared = sh_mine[...].astype(F32) + sh_other[...].astype(F32)
    routed_sum = own_sum[...]
    for j in range(1, outer):
        sum_copy(j).wait_recv()
        routed_sum = routed_sum + sums_in[j].astype(F32)
    routed[tp] = routed_sum.astype(BF16)
    routed_copy = pair(2, routed.at[tp], routed.at[tp])
    routed_copy.start()
    routed_copy.wait()
    total = jnp.concatenate([routed[0], routed[1]], axis=1).astype(F32) + shared
    out_ref[...] = (middle.astype(F32) + rms_norm(total, g_ffn_out[...])).astype(BF16)
    for j in range(outer):
        if j > 0:
            info_copy(j).wait_send()
            line_copy(j).wait_send()
            sum_copy(j).wait_send()
        part_copy(j).wait_send()
        each(0, lambda i: forward(j, i).wait_send())
        each(1, lambda i: to_ep(j, i).wait_send())
        each(1, lambda i: to_back(j, i).wait_send())


def tail(layer_out, state, inflow, window, out_ref, state_ref, window_ref):
    out_ref[...] = layer_out[...]
    state_ref[...] = state[...]
    taken = window.shape[0]
    for j in range(taken - 1):
        window_ref[j] = window[j + 1]
    window_ref[taken - 1] = inflow[...]


def on_device(
    tokens,
    lru_state,
    conv_window,
    gain_mix_in,
    gain_mix_out,
    gain_ffn_in,
    gain_ffn_out,
    w_branch,
    w_input,
    conv_taps,
    gate_a,
    gate_x,
    decay_rate,
    w_mix_out,
    routes,
    route_weight,
    expert_gate,
    expert_up,
    expert_down,
    shared_gate,
    shared_up,
    shared_down,
):
    n_ep = lax.axis_size("ep")
    count, width = tokens.shape
    share = width // 2
    local_ch = lru_state.shape[1]
    capacity = max(2, 2 * count * routes.shape[1] // (n_ep * expert_gate.shape[0]))
    cap = -(-capacity // 16) * 16
    slots = n_ep * cap
    outer = 1
    while outer * outer * 4 <= n_ep and n_ep % (2 * outer) == 0:
        outer *= 2
    inner = n_ep // outer
    vmem = pl.BlockSpec(memory_space=pltpu.VMEM)
    hbm = pl.BlockSpec(memory_space=pl.ANY)
    window = jnp.transpose(conv_window, (1, 0, 2))
    args = (
        (tokens, hbm),
        (lru_state, hbm),
        (window, hbm),
        (gain_mix_in[None], vmem),
        (gain_mix_out[None], vmem),
        (gain_ffn_in[None], vmem),
        (gain_ffn_out[None], vmem),
        (w_branch, hbm),
        (w_input, hbm),
        (conv_taps, vmem),
        (gate_a, hbm),
        (gate_x, hbm),
        (decay_rate[None], vmem),
        (w_mix_out, hbm),
        (routes.T, vmem),
        (route_weight.T, vmem),
        (expert_gate[0], hbm),
        (expert_up[0], hbm),
        (expert_down[0], hbm),
        (shared_gate, hbm),
        (shared_up, hbm),
        (shared_down, hbm),
    )
    held = lambda a: pltpu.VMEM(a.shape, a.dtype)
    dma = pltpu.SemaphoreType.DMA
    layer_out, new_state, inflow = pl.pallas_call(
        functools.partial(kernel, outer, inner, cap),
        out_shape=(
            jax.ShapeDtypeStruct((count, width), BF16),
            jax.ShapeDtypeStruct((count, local_ch), F32),
            jax.ShapeDtypeStruct((count, local_ch), BF16),
        ),
        in_specs=[spec for _, spec in args],
        out_specs=(vmem, vmem, vmem),
        scratch_shapes=[
            held(tokens),
            held(lru_state),
            held(window),
            held(w_branch),
            held(w_input),
            held(gate_a),
            held(gate_x),
            held(w_mix_out),
            held(expert_gate[0]),
            held(expert_up[0]),
            held(expert_down[0]),
            held(shared_gate),
            held(shared_up),
            held(shared_down),
            pltpu.VMEM((count, width), BF16),
            pltpu.VMEM((count, width), BF16),
            pltpu.VMEM((count, width), BF16),
            pltpu.VMEM((count, width), BF16),
            pltpu.VMEM((2, count, share), BF16),
            pltpu.VMEM((outer, -(-2 * routes.shape[1] // 8) * 8, -(-count // 128) * 128), F32),
            pltpu.VMEM((outer, count, share), BF16),
            pltpu.VMEM((slots, share), BF16),
            pltpu.VMEM((2, slots, share), BF16),
            pltpu.VMEM((slots, share), BF16),
            pltpu.VMEM((slots, share), BF16),
            pltpu.VMEM((slots, share), BF16),
            pltpu.VMEM((slots, share), BF16),
            pltpu.VMEM((slots, share), BF16),
            pltpu.VMEM((outer, count, share), BF16),
            pltpu.VMEM((outer, count, share), BF16),
            pltpu.VMEM((count, share), F32),
            pltpu.VMEM((2, count, share), BF16),
            dma((14,)),
            dma((3,)),
            dma((3,)),
            dma((n_ep,)),
            dma((n_ep,)),
            dma((n_ep,)),
            dma((n_ep,)),
            dma((n_ep,)),
            dma((n_ep,)),
        ]
        + [dma((outer,))] * 8,
        compiler_params=pltpu.CompilerParams(
            collective_id=0, has_side_effects=True, vmem_limit_bytes=60 * 1024 * 1024
        ),
        name="layer",
    )(*[value for value, _ in args])
    layer_out, new_state, new_window = pl.pallas_call(
        tail,
        out_shape=(
            jax.ShapeDtypeStruct((count, width), BF16),
            jax.ShapeDtypeStruct((count, local_ch), F32),
            jax.ShapeDtypeStruct(window.shape, BF16),
        ),
        in_specs=[vmem] * 4,
        out_specs=(vmem,) * 3,
        name="hand_over",
    )(layer_out, new_state, inflow, window)
    return (layer_out, new_state, jnp.transpose(new_window, (1, 0, 2)))


def solution(mesh):
    placed = (
        P("ep", None),
        P("ep", "tp"),
        P("ep", None, "tp"),
        P(),
        P(),
        P(),
        P(),
        P(None, "tp"),
        P(None, "tp"),
        P(None, "tp"),
        P("tp", None, None),
        P("tp", None, None),
        P("tp"),
        P("tp", None),
        P("ep", None),
        P("ep", None),
        P("ep", None, "tp"),
        P("ep", None, "tp"),
        P("ep", "tp", None),
        P(None, "tp"),
        P(None, "tp"),
        P("tp", None),
    )
    return jax.shard_map(
        on_device,
        mesh=mesh,
        in_specs=placed,
        out_specs=(P("ep", None), P("ep", "tp"), P("ep", None, "tp")),
        check_vma=False,
    )
```

time: 49.8 us -> 40.8 us (0.82)
  the two profiles are of different devices: /device:TPU:29 before, /device:TPU:0 now
where the time goes in v2:
time: 40.8 us; the launch traced here: 40.6 us
  Pallas kernels  39.9 us (98%)
  between operations  0.65 us (2%)
    pallas_call x1, Pallas kernels, on_device(): pl.pallas_call(functools.partial(kernel, outer, inner, cap), out_shape=(j...  38.2 us
    pallas_call x1, Pallas kernels, on_device(): pl.pallas_call(tail, out_shape=(jax.ShapeDtypeStruct((count, width), BF16...  1.73 us

profile of v2, /device:TPU:0, one launch (start us, length us, event | category | flops | bytes accessed | tf_op | source)
XLA Modules:
  0.0 40.6 jit_solution(17895827659493150804)
XLA Ops:
  0.6 38.2 %layer.1 = (bf16[32,2048]{1,0:T(8,128)(2,1)}, f32[32,512]{1,0:T(8,128)}, bf16[32,512]{1,0:T(8,128)(2,1)}) custom-call(bf16[32,2048]{1,0:T(8,128)(2,1)} %tokens_h.1, f32[32,512]{1,0:T(8,128)} %lru_h.1, bf16[3,32,512]{2,1,0:T(8,128)(2,1)} %bitcast.15, f32[1,2048]{1,0:T(1,128)} %bitcast.17, f32[1,2048]{1,0:T(1,128)} %bitcast.18, f32[1,2048]{1,0:T(1,128)} %bitcast.19, ...), custom_call_target="tpu_custom_call" | custom-call | tf_op jit(solution)/shard_map/layer/pallas_call | solution.py:492
  38.8 1.7 %hand_over.1 = (bf16[32,2048]{1,0:T(8,128)(2,1)}, f32[32,512]{1,0:T(8,128)}, bf16[3,32,512]{2,1,0:T(8,128)(2,1)}) custom-call(bf16[32,2048]{1,0:T(8,128)(2,1)} %get-tuple-element.9.layer_out, f32[32,512]{1,0:T(8,128)} %get-tuple-element.10.state, bf16[32,512]{1,0:T(8,128)(2,1)} %get-tuple-element.11.inflow, bf16[3,32,512]{2,1,0:T(8,128)(2,1)} %bitcast.16), custom_call_target="tpu_custom_call" | custom-call | tf_op jit(solution)/shard_map/hand_over/pallas_call | solution.py:550
